TPU v7x, 32 devices: a whole 2x2x4 slice. The times are simulated.
32 devices in a mesh: ra: 4 (over z), cb: 4 (over y, x), dp: 2 (over core).
Axes of the slice: x: 2, y: 2, z: 4, core: 2. Of those that a mesh axis runs over, the one named last changes fastest.
Arguments:
- stream: bfloat16 [3072, 4096], P(('cb', 'dp'), 'ra'), may hold values from -20 to 20
- up_first: bfloat16 [4096, 16384], P('cb', 'ra'), may hold values from -0.09375 to 0.09375
- down_first: bfloat16 [16384, 4096], P('ra', 'cb'), may hold values from -0.046875 to 0.046875
- up_second: bfloat16 [4096, 16384], P('cb', 'ra'), may hold values from -0.09375 to 0.09375
- down_second: bfloat16 [16384, 4096], P('ra', 'cb'), may hold values from -0.046875 to 0.046875
- gain_first: float32 [4096], P('ra'), may hold values from 0.1 to 1.9
- bias_first: float32 [4096], P('ra'), may hold values from -3 to 3
- gain_second: float32 [4096], P('ra'), may hold values from 0.1 to 1.9
- bias_second: float32 [4096], P('ra'), may hold values from -3 to 3
Outputs:
- result: bfloat16 [3072, 4096], P(('cb', 'dp'), 'ra')
All inputs are finite; a program needn't handle non-finite values.
Results may differ from a plain program's by a relative error of at most 0.0093.
Values may be sent and summed in bfloat16 or wider, within the bound.
A program may use at most 192 MiB of HBM per device.

v0:
```python
import jax
import jax.numpy as jnp
from jax import lax
from jax.sharding import PartitionSpec as P

RESID = 1.4142135
EPS = 0.5


def sublayer(x, up, down, gain, bias):
    whole = lax.all_gather(x, "ra", axis=1, tiled=True)
    pre = jnp.dot(
        whole, lax.all_gather(up, "cb", axis=0, tiled=True), preferred_element_type=jnp.float32
    )
    hidden = jnp.square(jax.nn.relu(pre)).astype(jnp.bfloat16)
    partial_sums = jnp.dot(
        hidden, lax.all_gather(down, "cb", axis=1, tiled=True), preferred_element_type=jnp.float32
    )
    branch = lax.psum_scatter(partial_sums, "ra", scatter_dimension=1, tiled=True)
    mixed = RESID * x.astype(jnp.float32) + branch
    width = mixed.shape[1] * lax.axis_size("ra")
    total, squares = lax.psum(
        (jnp.sum(mixed, axis=1, keepdims=True), jnp.sum(mixed * mixed, axis=1, keepdims=True)), "ra"
    )
    mean = total / width
    var = squares / width - mean * mean
    centered = mixed - mean
    return (centered * lax.rsqrt(var + EPS) * gain + bias).astype(jnp.bfloat16)


def body(
    stream,
    up_first,
    down_first,
    up_second,
    down_second,
    gain_first,
    bias_first,
    gain_second,
    bias_second,
):
    x = stream
    for up, down, gain, bias in (
        (up_first, down_first, gain_first, bias_first),
        (up_second, down_second, gain_second, bias_second),
    ):
        x = sublayer(x, up, down, gain, bias)
    return x


def solution(mesh):
    placed = (
        P(("cb", "dp"), "ra"),
        P("cb", "ra"),
        P("ra", "cb"),
        P("cb", "ra"),
        P("ra", "cb"),
        P("ra"),
        P("ra"),
        P("ra"),
        P("ra"),
    )
    return jax.shard_map(
        body, mesh=mesh, in_specs=placed, out_specs=P(("cb", "dp"), "ra"), check_vma=False
    )
```

profile of v0, /device:TPU:0, one launch (start us, length us, event | category | flops | bytes accessed | tf_op | source)
XLA Modules:
  0.0 1616.1 jit_solution(16480345639922610143)
XLA Ops:
  6.5 0.0 all-gather.7.cloned.1.call-start
  6.5 0.7 all-gather.7.cloned.1.call-update
  7.3 0.0 all-gather.9.cloned.1.call-start
  7.3 0.7 all-gather.9.cloned.1.call-update
  8.0 0.0 all-gather.11.cloned.1.call-start
  8.1 0.7 all-gather.11.cloned.1.call-update
  8.7 0.0 reduce-scatter.3.cloned.1.call-start
  8.8 66.3 %all-gather.7.cloned.1.call-done = bf16[384,4096]{1,0:T(8,128)(2,1)} async-done(((bf16[384,1024]{1,0:T(8,128)(2,1)}), bf16[384,4096]{1,0:T(8,128)(2,1)}) %all-gather.7.cloned.1.call-update) | async-done | bytes 3145744 | tf_op jit(solution)/shard_map/all_gather | solution.py:11
  75.1 297.6 %all-gather.9.cloned.1.call-done = bf16[4096,4096]{1,0:T(8,128)(2,1)} async-done(((bf16[1024,4096]{1,0:T(8,128)(2,1)}), bf16[4096,4096]{1,0:T(8,128)(2,1)}) %all-gather.9.cloned.1.call-update) | async-done | bytes 33554448 | tf_op jit(solution)/shard_map/all_gather | solution.py:13
  372.7 21.7 %fusion.37 = bf16[384,4096]{1,0:T(8,128)(2,1)S(1)} fusion(bf16[4096,4096]{1,0:T(8,128)(2,1)} %all-gather.9.cloned.1.call-done, bf16[384,4096]{1,0:T(8,128)(2,1)} %all-gather.7.cloned.1.call-done), kind=kOutput, calls=%bitcast_fusion.2.clone.1 | convolution fusion | flops 12889620480 | bytes 39845888 | tf_op jit(solution)/shard_map/dot_general | solution.py:12
  394.4 277.2 %all-gather.11.cloned.1.call-done = bf16[4096,4096]{1,0:T(8,128)(2,1)} async-done(((bf16[4096,1024]{1,0:T(8,128)(2,1)}), bf16[4096,4096]{1,0:T(8,128)(2,1)}) %all-gather.11.cloned.1.call-update) | async-done | bytes 33554448 | tf_op jit(solution)/shard_map/all_gather | solution.py:17
  671.7 19.7 %fusion.2 = f32[384,4096]{1,0:T(8,128)} fusion(bf16[4096,4096]{1,0:T(8,128)(2,1)} %all-gather.11.cloned.1.call-done, bf16[384,4096]{1,0:T(8,128)(2,1)S(1)} %fusion.37), kind=kOutput, calls=%fused_computation.14 | convolution fusion | flops 12884901888 | bytes 42991616 | tf_op jit(solution)/shard_map/dot_general | solution.py:16
  691.4 0.0 reduce-scatter.3.cloned.1.call-update
  691.4 0.0 copy-start.1
  691.4 0.0 copy-start.4
  691.4 0.0 copy-start.5
  691.4 0.0 all-gather.15.cloned.1.call-start
  691.5 0.5 all-gather.15.cloned.1.call-update
  692.0 0.0 all-gather.13.cloned.1.call-start
  692.1 110.3 %reduce-scatter.3.cloned.1.call-done = f32[384,1024]{1,0:T(8,128)} async-done(((f32[384,4096]{1,0:T(8,128)}), f32[384,1024]{1,0:T(8,128)}) %reduce-scatter.3.cloned.1.call-update) | async-done | bytes 1572880 | tf_op jit(solution)/shard_map/reduce_scatter | solution.py:19
  802.3 0.0 copy-done.1
  802.3 0.0 copy-start.2
  802.3 1.9 fusion
  804.3 11.0 all-reduce.1
  815.3 0.0 copy-done.4
  815.3 0.0 copy-done.5
  815.3 0.0 copy-done.2
  815.3 1.3 add_convert_fusion.1
  816.6 0.0 all-gather.13.cloned.1.call-update
  816.7 0.0 all-gather.17.cloned.1.call-start
  816.7 0.7 all-gather.17.cloned.1.call-update
  817.4 0.2 reduce-scatter.5.cloned.1.call-start
  817.7 284.0 %all-gather.15.cloned.1.call-done = bf16[4096,4096]{1,0:T(8,128)(2,1)} async-done(((bf16[1024,4096]{1,0:T(8,128)(2,1)}), bf16[4096,4096]{1,0:T(8,128)(2,1)}) %all-gather.15.cloned.1.call-update) | async-done | bytes 33554448 | tf_op jit(solution)/shard_map/all_gather | solution.py:13
  1101.7 64.9 %all-gather.13.cloned.1.call-done = bf16[384,4096]{1,0:T(8,128)(2,1)} async-done(((bf16[384,1024]{1,0:T(8,128)(2,1)}), bf16[384,4096]{1,0:T(8,128)(2,1)}) %all-gather.13.cloned.1.call-update) | async-done | bytes 3145744 | tf_op jit(solution)/shard_map/all_gather | solution.py:11
  1166.6 22.8 %fusion.41 = bf16[384,4096]{1,0:T(8,128)(2,1)S(1)} fusion(bf16[4096,4096]{1,0:T(8,128)(2,1)} %all-gather.15.cloned.1.call-done, bf16[384,4096]{1,0:T(8,128)(2,1)} %all-gather.13.cloned.1.call-done), kind=kOutput, calls=%bitcast_fusion.3.clone | convolution fusion | flops 12889620480 | bytes 39845888 | tf_op jit(solution)/shard_map/dot_general | solution.py:12
  1189.4 274.8 %all-gather.17.cloned.1.call-done = bf16[4096,4096]{1,0:T(8,128)(2,1)} async-done(((bf16[4096,1024]{1,0:T(8,128)(2,1)}), bf16[4096,4096]{1,0:T(8,128)(2,1)}) %all-gather.17.cloned.1.call-update) | async-done | bytes 33554448 | tf_op jit(solution)/shard_map/all_gather | solution.py:17
  1464.2 19.8 %fusion.3 = f32[384,4096]{1,0:T(8,128)} fusion(bf16[4096,4096]{1,0:T(8,128)(2,1)} %all-gather.17.cloned.1.call-done, bf16[384,4096]{1,0:T(8,128)(2,1)S(1)} %fusion.41), kind=kOutput, calls=%fused_computation.15 | convolution fusion | flops 12884901888 | bytes 42991616 | tf_op jit(solution)/shard_map/dot_general | solution.py:16
  1483.9 0.0 copy-start
  1483.9 0.0 copy-start.6
  1483.9 0.0 copy-start.7
  1484.0 0.0 reduce-scatter.5.cloned.1.call-update
  1484.0 110.9 %reduce-scatter.5.cloned.1.call-done = f32[384,1024]{1,0:T(8,128)} async-done(((f32[384,4096]{1,0:T(8,128)}), f32[384,1024]{1,0:T(8,128)}) %reduce-scatter.5.cloned.1.call-update) | async-done | bytes 1572880 | tf_op jit(solution)/shard_map/reduce_scatter | solution.py:19
  1594.9 0.0 copy-done
  1594.9 0.0 copy-start.3
  1594.9 1.9 fusion.1
  1596.9 11.0 all-reduce
  1607.9 0.0 copy-done.6
  1607.9 0.0 copy-done.7
  1607.9 0.0 copy-done.3
  1607.9 1.3 add_convert_fusion
  (6 shorter events, 0.1 us)
Async XLA Ops:
  6.5 68.6 %all-gather.7.cloned.1.call-start = ((), (), s32[]{:S(2)}) async-start(), calls=%async_computation.2 | async-start | bytes 3932160 | tf_op jit(solution)/shard_map/all_gather | solution.py:11
  7.3 365.4 %all-gather.9.cloned.1.call-start = ((), (), s32[]{:S(2)}) async-start(), calls=%async_computation.3 | async-start | bytes 41943040 | tf_op jit(solution)/shard_map/all_gather | solution.py:13
  8.0 663.7 %all-gather.11.cloned.1.call-start = ((), (), s32[]{:S(2)}) async-start(), calls=%async_computation.4 | async-start | bytes 41943040 | tf_op jit(solution)/shard_map/all_gather | solution.py:17
  8.7 793.6 %reduce-scatter.3.cloned.1.call-start = ((), (), s32[]{:S(2)}) async-start(), calls=%async_computation.5 | async-start | bytes 7864320 | tf_op jit(solution)/shard_map/reduce_scatter | solution.py:19
  691.4 110.9 %copy-start.1 = (bf16[384,1024]{1,0:T(8,128)(2,1)S(1)}, bf16[384,1024]{1,0:T(8,128)(2,1)}, u32[]{:S(2)}) copy-start(bf16[384,1024]{1,0:T(8,128)(2,1)} %param.9) | copy-start | bytes 2359300
  691.4 123.9 %copy-start.4 = (f32[1024]{0:T(1024)S(1)}, f32[1024]{0:T(1024)}, u32[]{:S(2)}) copy-start(f32[1024]{0:T(1024)} %param.15) | copy-start | bytes 12292
  691.4 123.9 %copy-start.5 = (f32[1024]{0:T(1024)S(1)}, f32[1024]{0:T(1024)}, u32[]{:S(2)}) copy-start(f32[1024]{0:T(1024)} %param.14) | copy-start | bytes 12292
  691.4 410.2 %all-gather.15.cloned.1.call-start = ((), (), s32[]{:S(2)}) async-start(), calls=%async_computation.7 | async-start | bytes 41943040 | tf_op jit(solution)/shard_map/all_gather | solution.py:13
  692.0 474.5 %all-gather.13.cloned.1.call-start = ((), (), s32[]{:S(2)}) async-start(), calls=%async_computation.6 | async-start | bytes 3932160 | tf_op jit(solution)/shard_map/all_gather | solution.py:11
  802.3 13.0 copy-start.2
  816.7 647.5 %all-gather.17.cloned.1.call-start = ((), (), s32[]{:S(2)}) async-start(), calls=%async_computation.8 | async-start | bytes 41943040 | tf_op jit(solution)/shard_map/all_gather | solution.py:17
  817.4 777.5 %reduce-scatter.5.cloned.1.call-start = ((), (), s32[]{:S(2)}) async-start(), calls=%async_computation.9 | async-start | bytes 7864320 | tf_op jit(solution)/shard_map/reduce_scatter | solution.py:19
  1483.9 111.0 %copy-start = (bf16[384,1024]{1,0:T(8,128)(2,1)S(1)}, bf16[384,1024]{1,0:T(8,128)(2,1)}, u32[]{:S(2)}) copy-start(bf16[384,1024]{1,0:T(8,128)(2,1)} %add_convert_fusion.1) | copy-start | bytes 2359300
  1483.9 123.9 %copy-start.6 = (f32[1024]{0:T(1024)S(1)}, f32[1024]{0:T(1024)}, u32[]{:S(2)}) copy-start(f32[1024]{0:T(1024)} %param.17) | copy-start | bytes 12292
  1483.9 123.9 %copy-start.7 = (f32[1024]{0:T(1024)S(1)}, f32[1024]{0:T(1024)}, u32[]{:S(2)}) copy-start(f32[1024]{0:T(1024)} %param.16) | copy-start | bytes 12292
  1594.9 13.0 copy-start.3
Sparse Core Ops, SparseCore 0:
  8.9 66.1 all-gather.6
  76.9 295.7 all-gather.8
  374.6 297.0 all-gather.10
  691.5 110.7 reduce-scatter.2
  804.0 297.5 all-gather.14
  1103.1 63.4 all-gather.12
  1168.4 295.7 all-gather.16
  1484.1 110.7 reduce-scatter.4
where the time goes:
time: 1620 us
  waiting for transfers between devices  1490 us (92%)
  matrix products  84 us (5%)
  blocking collectives  21.9 us (1%)
    all_gather x2, waiting for transfers between devices, sublayer(): lax.all_gather(up, 'cb', axis=0, tiled=True)  582 us
    all_gather x2, waiting for transfers between devices, sublayer(): lax.all_gather(down, 'cb', axis=1, tiled=True)  552 us
    reduce_scatter x2, waiting for transfers between devices, sublayer(): lax.psum_scatter(partial_sums, 'ra', scatter_dimension=1, tiled=True)  221 us
    all_gather x2, waiting for transfers between devices, sublayer(): whole = lax.all_gather(x, 'ra', axis=1, tiled=True)  131 us
    dot_general x2, matrix products, sublayer(): jnp.dot(whole, lax.all_gather(up, 'cb', axis=0, tiled=True), preferred_el...  44.5 us
    dot_general x2, matrix products, sublayer(): jnp.dot(hidden, lax.all_gather(down, 'cb', axis=1, tiled=True), preferred...  39.5 us
  transfers between devices with their start and end apart: 8, of which 8 were waited for; matrix products, arithmetic and copies ran while one was open for 3% of the time, Pallas kernels for 0%

commit v1 on v0

--- a/solution.py
+++ b/solution.py
@@ -8,7 +8,12 @@
 
 
 def sublayer(x, up, down, gain, bias):
-    whole = lax.all_gather(x, "ra", axis=1, tiled=True)
+    ring = [x]
+    for hop in range(3):
+        ring.append(lax.ppermute(ring[-1], "ra", [(dev, (dev + 1) % 4) for dev in range(4)]))
+    whole = jnp.roll(
+        jnp.concatenate(ring[::-1], axis=1), (lax.axis_index("ra") + 1) * ring[0].shape[1], axis=1
+    )
     pre = jnp.dot(
         whole, lax.all_gather(up, "cb", axis=0, tiled=True), preferred_element_type=jnp.float32
     )

time: 1620 us -> 1490 us (0.920)
  waiting for transfers between devices: 1490 us -> 1350 us
    all_gather x2 -> x0, waiting for transfers between devices: 131 us -> none  [sublayer(): whole = lax.all_gather(x, 'ra', axis=1, tiled=True)]
    ppermute x0 -> x6, waiting for transfers between devices: none -> 97.6 us  [sublayer(): lax.ppermute(ring[-1], 'ra', [(dev, (dev + 1) % 4) for dev in range(4)])]
    all_gather x2, waiting for transfers between devices: 582 us -> 484 us  [sublayer(): lax.all_gather(up, 'cb', axis=0, tiled=True)]
  transfers between devices with their start and end apart: 8 -> 12, of which waited for: 8 -> 11; matrix products, arithmetic and copies ran while one was open for 3% -> 4% of each run, Pallas kernels for 0% -> 0%
where the time goes in v1:
time: 1490 us
  waiting for transfers between devices  1350 us (91%)
  matrix products  99.5 us (7%)
  blocking collectives  21.9 us (1%)
    all_gather x2, waiting for transfers between devices, sublayer(): lax.all_gather(down, 'cb', axis=1, tiled=True)  542 us
    all_gather x2, waiting for transfers between devices, sublayer(): lax.all_gather(up, 'cb', axis=0, tiled=True)  484 us
    reduce_scatter x2, waiting for transfers between devices, sublayer(): lax.psum_scatter(partial_sums, 'ra', scatter_dimension=1, tiled=True)  221 us
    ppermute x6, waiting for transfers between devices, sublayer(): lax.ppermute(ring[-1], 'ra', [(dev, (dev + 1) % 4) for dev in range(4)])  97.6 us
    dot_general x2, matrix products, sublayer(): jnp.dot(whole, lax.all_gather(up, 'cb', axis=0, tiled=True), preferred_el...  56.3 us
    dot_general x2, matrix products, sublayer(): jnp.dot(hidden, lax.all_gather(down, 'cb', axis=1, tiled=True), preferred...  43.2 us
  transfers between devices with their start and end apart: 12, of which 11 were waited for; matrix products, arithmetic and copies ran while one was open for 4% of the time, Pallas kernels for 0%

profile of v1, /device:TPU:0, one launch (start us, length us, event | category | flops | bytes accessed | tf_op | source)
XLA Modules:
  0.0 1493.7 jit_solution(16241074446072122666)
XLA Ops:
  6.5 0.0 copy-start
  6.5 0.0 all-gather.5.cloned.1.call-start
  6.5 0.7 all-gather.5.cloned.1.call-update
  7.3 0.0 all-gather.7.cloned.1.call-start
  7.3 0.7 all-gather.7.cloned.1.call-update
  8.0 0.0 reduce-scatter.3.cloned.1.call-start
  8.1 0.0 copy-done
  8.1 3.1 collective-permute-start
  11.2 19.6 %collective-permute-done = bf16[384,1024]{1,0:T(8,128)(2,1)S(1)} collective-permute-done((bf16[384,1024]{1,0:T(8,128)(2,1)S(1)}, bf16[384,1024]{1,0:T(8,128)(2,1)S(1)}, u32[]{:S(2)}, u32[]{:S(2)}) %collective-permute-start) | collective-permute-done | bytes 786464 | tf_op jit(solution)/shard_map/ppermute | solution.py:13
  30.7 0.0 collective-permute-start.1
  30.7 20.5 %collective-permute-done.1 = bf16[384,1024]{1,0:T(8,128)(2,1)S(1)} collective-permute-done((bf16[384,1024]{1,0:T(8,128)(2,1)S(1)}, bf16[384,1024]{1,0:T(8,128)(2,1)S(1)}, u32[]{:S(2)}, u32[]{:S(2)}) %collective-permute-start.1) | collective-permute-done | bytes 786464 | tf_op jit(solution)/shard_map/ppermute | solution.py:13
  51.2 0.0 collective-permute-start.2
  51.2 19.6 %collective-permute-done.2 = bf16[384,1024]{1,0:T(8,128)(2,1)S(1)} collective-permute-done((bf16[384,1024]{1,0:T(8,128)(2,1)S(1)}, bf16[384,1024]{1,0:T(8,128)(2,1)S(1)}, u32[]{:S(2)}, u32[]{:S(2)}) %collective-permute-start.2) | collective-permute-done | bytes 786464 | tf_op jit(solution)/shard_map/ppermute | solution.py:13
  70.9 238.1 %all-gather.5.cloned.1.call-done = bf16[4096,4096]{1,0:T(8,128)(2,1)} async-done(((bf16[1024,4096]{1,0:T(8,128)(2,1)}), bf16[4096,4096]{1,0:T(8,128)(2,1)}) %all-gather.5.cloned.1.call-update) | async-done | bytes 33554448 | tf_op jit(solution)/shard_map/all_gather | solution.py:18
  309.0 28.1 %multiply_convert_fusion.1 = bf16[384,4096]{1,0:T(8,128)(2,1)} fusion(bf16[4096,4096]{1,0:T(8,128)(2,1)} %all-gather.5.cloned.1.call-done, s32[]{:T(128)S(6)} %select_n.13, bf16[384,1024]{1,0:T(8,128)(2,1)S(1)} %collective-permute-done.2, bf16[384,1024]{1,0:T(8,128)(2,1)S(1)} %collective-permute-done.1, bf16[384,1024]{1,0:T(8,128)(2,1)S(1)} %collective-permute-done, ...), kind=kOutput, calls=%fused_computation.17 | convolution fusion | flops 12914786304 | bytes 39845892 | tf_op jit(solution)/shard_map/dot_general | solution.py:17
  337.1 270.8 %all-gather.7.cloned.1.call-done = bf16[4096,4096]{1,0:T(8,128)(2,1)} async-done(((bf16[4096,1024]{1,0:T(8,128)(2,1)}), bf16[4096,4096]{1,0:T(8,128)(2,1)}) %all-gather.7.cloned.1.call-update) | async-done | bytes 33554448 | tf_op jit(solution)/shard_map/all_gather | solution.py:22
  608.0 21.7 %fusion.24 = f32[384,4096]{1,0:T(8,128)} fusion(bf16[384,4096]{1,0:T(8,128)(2,1)} %multiply_convert_fusion.1, bf16[4096,4096]{1,0:T(8,128)(2,1)} %all-gather.7.cloned.1.call-done), kind=kOutput, calls=%fused_computation.48 | convolution fusion | flops 12884901888 | bytes 42991616 | tf_op jit(solution)/shard_map/dot_general | solution.py:21
  629.7 0.0 reduce-scatter.3.cloned.1.call-update
  629.7 0.0 all-gather.9.cloned.1.call-start
  629.7 0.5 all-gather.9.cloned.1.call-update
  630.3 0.0 copy-start.1
  630.3 0.0 copy-start.2
  630.3 0.0 all-gather.11.cloned.1.call-start
  630.3 0.5 all-gather.11.cloned.1.call-update
  630.9 0.0 reduce-scatter.5.cloned.1.call-start
  630.9 109.7 %reduce-scatter.3.cloned.1.call-done = f32[384,1024]{1,0:T(8,128)} async-done(((f32[384,4096]{1,0:T(8,128)}), f32[384,1024]{1,0:T(8,128)}) %reduce-scatter.3.cloned.1.call-update) | async-done | bytes 1572880 | tf_op jit(solution)/shard_map/reduce_scatter | solution.py:24
  740.6 1.8 fusion.18
  742.5 11.0 all-reduce.1
  753.5 0.0 copy-done.1
  753.5 0.0 copy-done.2
  753.5 2.4 add_convert_fusion.1
  755.9 0.1 collective-permute-start.3
  756.0 19.3 %collective-permute-done.3 = bf16[384,1024]{1,0:T(8,128)(2,1)S(1)} collective-permute-done((bf16[384,1024]{1,0:T(8,128)(2,1)S(1)}, bf16[384,1024]{1,0:T(8,128)(2,1)S(1)}, u32[]{:S(2)}, u32[]{:S(2)}) %collective-permute-start.3) | collective-permute-done | bytes 786464 | tf_op jit(solution)/shard_map/ppermute | solution.py:13
  775.3 0.0 collective-permute-start.4
  775.3 18.5 %collective-permute-done.4 = bf16[384,1024]{1,0:T(8,128)(2,1)S(1)} collective-permute-done((bf16[384,1024]{1,0:T(8,128)(2,1)S(1)}, bf16[384,1024]{1,0:T(8,128)(2,1)S(1)}, u32[]{:S(2)}, u32[]{:S(2)}) %collective-permute-start.4) | collective-permute-done | bytes 786464 | tf_op jit(solution)/shard_map/ppermute | solution.py:13
  793.8 0.0 collective-permute-start.5
  793.8 246.1 %all-gather.9.cloned.1.call-done = bf16[4096,4096]{1,0:T(8,128)(2,1)} async-done(((bf16[1024,4096]{1,0:T(8,128)(2,1)}), bf16[4096,4096]{1,0:T(8,128)(2,1)}) %all-gather.9.cloned.1.call-update) | async-done | bytes 33554448 | tf_op jit(solution)/shard_map/all_gather | solution.py:18
  1039.9 0.0 collective-permute-done.5
  1040.0 28.1 %multiply_convert_fusion = bf16[384,4096]{1,0:T(8,128)(2,1)} fusion(bf16[4096,4096]{1,0:T(8,128)(2,1)} %all-gather.9.cloned.1.call-done, s32[]{:T(128)S(6)} %select_n.13, bf16[384,1024]{1,0:T(8,128)(2,1)S(1)} %collective-permute-done.5, bf16[384,1024]{1,0:T(8,128)(2,1)S(1)} %collective-permute-done.4, bf16[384,1024]{1,0:T(8,128)(2,1)S(1)} %collective-permute-done.3, ...), kind=kOutput, calls=%fused_computation.16 | convolution fusion | flops 12914786304 | bytes 39845892 | tf_op jit(solution)/shard_map/dot_general | solution.py:17
  1068.1 270.7 %all-gather.11.cloned.1.call-done = bf16[4096,4096]{1,0:T(8,128)(2,1)} async-done(((bf16[4096,1024]{1,0:T(8,128)(2,1)}), bf16[4096,4096]{1,0:T(8,128)(2,1)}) %all-gather.11.cloned.1.call-update) | async-done | bytes 33554448 | tf_op jit(solution)/shard_map/all_gather | solution.py:22
  1338.8 21.6 %fusion.25 = f32[384,4096]{1,0:T(8,128)} fusion(bf16[384,4096]{1,0:T(8,128)(2,1)} %multiply_convert_fusion, bf16[4096,4096]{1,0:T(8,128)(2,1)} %all-gather.11.cloned.1.call-done), kind=kOutput, calls=%fused_computation.49 | convolution fusion | flops 12884901888 | bytes 42991616 | tf_op jit(solution)/shard_map/dot_general | solution.py:21
  1360.3 0.0 copy-start.3
  1360.3 0.0 copy-start.4
  1360.3 0.0 reduce-scatter.5.cloned.1.call-update
  1360.4 110.9 %reduce-scatter.5.cloned.1.call-done = f32[384,1024]{1,0:T(8,128)} async-done(((f32[384,4096]{1,0:T(8,128)}), f32[384,1024]{1,0:T(8,128)}) %reduce-scatter.5.cloned.1.call-update) | async-done | bytes 1572880 | tf_op jit(solution)/shard_map/reduce_scatter | solution.py:24
  1471.3 1.8 fusion.19
  1473.1 11.0 all-reduce
  1484.1 0.0 copy-done.3
  1484.1 0.0 copy-done.4
  1484.2 2.7 add_convert_fusion
  (6 shorter events, 0.1 us)
Async XLA Ops:
  6.5 1.5 copy-start
  6.5 302.5 %all-gather.5.cloned.1.call-start = ((), (), s32[]{:S(2)}) async-start(), calls=%async_computation.2 | async-start | bytes 41943040 | tf_op jit(solution)/shard_map/all_gather | solution.py:18
  7.3 600.7 %all-gather.7.cloned.1.call-start = ((), (), s32[]{:S(2)}) async-start(), calls=%async_computation.3 | async-start | bytes 41943040 | tf_op jit(solution)/shard_map/all_gather | solution.py:22
  8.0 732.6 %reduce-scatter.3.cloned.1.call-start = ((), (), s32[]{:S(2)}) async-start(), calls=%async_computation.4 | async-start | bytes 7864320 | tf_op jit(solution)/shard_map/reduce_scatter | solution.py:24
  8.1 22.7 %collective-permute-start = (bf16[384,1024]{1,0:T(8,128)(2,1)S(1)}, bf16[384,1024]{1,0:T(8,128)(2,1)S(1)}, u32[]{:S(2)}, u32[]{:S(2)}) collective-permute-start(bf16[384,1024]{1,0:T(8,128)(2,1)S(1)} %copy-done), channel_id=1, source_target_pairs={{0,8},{8,16},{16,24},{24,0},{1,9},{9,17},{17,25},{25,1},{2,10},{10... | collective-permute-start | bytes 2359304 | tf_op jit(solution)/shard_map/ppermute | solution.py:13
  30.7 20.5 %collective-permute-start.1 = (bf16[384,1024]{1,0:T(8,128)(2,1)S(1)}, bf16[384,1024]{1,0:T(8,128)(2,1)S(1)}, u32[]{:S(2)}, u32[]{:S(2)}) collective-permute-start(bf16[384,1024]{1,0:T(8,128)(2,1)S(1)} %collective-permute-done), channel_id=1, source_target_pairs={{0,8},{8,16},{16,24},{24,0},{1,9},{9,17},{17,25},{25,1},{2,10},{10... | collective-permute-start | bytes 2359304 | tf_op jit(solution)/shard_map/ppermute | solution.py:13
  51.2 19.6 %collective-permute-start.2 = (bf16[384,1024]{1,0:T(8,128)(2,1)S(1)}, bf16[384,1024]{1,0:T(8,128)(2,1)S(1)}, u32[]{:S(2)}, u32[]{:S(2)}) collective-permute-start(bf16[384,1024]{1,0:T(8,128)(2,1)S(1)} %collective-permute-done.1), channel_id=1, source_target_pairs={{0,8},{8,16},{16,24},{24,0},{1,9},{9,17},{17,25},{25,1},{2,10},{10... | collective-permute-start | bytes 2359304 | tf_op jit(solution)/shard_map/ppermute | solution.py:13
  629.7 410.3 %all-gather.9.cloned.1.call-start = ((), (), s32[]{:S(2)}) async-start(), calls=%async_computation.5 | async-start | bytes 41943040 | tf_op jit(solution)/shard_map/all_gather | solution.py:18
  630.3 123.2 %copy-start.1 = (f32[1024]{0:T(1024)S(1)}, f32[1024]{0:T(1024)}, u32[]{:S(2)}) copy-start(f32[1024]{0:T(1024)} %param.17) | copy-start | bytes 12292
  630.3 123.2 %copy-start.2 = (f32[1024]{0:T(1024)S(1)}, f32[1024]{0:T(1024)}, u32[]{:S(2)}) copy-start(f32[1024]{0:T(1024)} %param.16) | copy-start | bytes 12292
  630.3 708.5 %all-gather.11.cloned.1.call-start = ((), (), s32[]{:S(2)}) async-start(), calls=%async_computation.6 | async-start | bytes 41943040 | tf_op jit(solution)/shard_map/all_gather | solution.py:22
  630.9 840.4 %reduce-scatter.5.cloned.1.call-start = ((), (), s32[]{:S(2)}) async-start(), calls=%async_computation.7 | async-start | bytes 7864320 | tf_op jit(solution)/shard_map/reduce_scatter | solution.py:24
  755.9 19.4 %collective-permute-start.3 = (bf16[384,1024]{1,0:T(8,128)(2,1)S(1)}, bf16[384,1024]{1,0:T(8,128)(2,1)S(1)}, u32[]{:S(2)}, u32[]{:S(2)}) collective-permute-start(bf16[384,1024]{1,0:T(8,128)(2,1)S(1)} %add_convert_fusion.1), channel_id=1, source_target_pairs={{0,8},{8,16},{16,24},{24,0},{1,9},{9,17},{17,25},{25,1},{2,10},{10... | collective-permute-start | bytes 2359304 | tf_op jit(solution)/shard_map/ppermute | solution.py:13
  775.3 18.5 %collective-permute-start.4 = (bf16[384,1024]{1,0:T(8,128)(2,1)S(1)}, bf16[384,1024]{1,0:T(8,128)(2,1)S(1)}, u32[]{:S(2)}, u32[]{:S(2)}) collective-permute-start(bf16[384,1024]{1,0:T(8,128)(2,1)S(1)} %collective-permute-done.3), channel_id=1, source_target_pairs={{0,8},{8,16},{16,24},{24,0},{1,9},{9,17},{17,25},{25,1},{2,10},{10... | collective-permute-start | bytes 2359304 | tf_op jit(solution)/shard_map/ppermute | solution.py:13
  793.8 246.1 %collective-permute-start.5 = (bf16[384,1024]{1,0:T(8,128)(2,1)S(1)}, bf16[384,1024]{1,0:T(8,128)(2,1)S(1)}, u32[]{:S(2)}, u32[]{:S(2)}) collective-permute-start(bf16[384,1024]{1,0:T(8,128)(2,1)S(1)} %collective-permute-done.4), channel_id=1, source_target_pairs={{0,8},{8,16},{16,24},{24,0},{1,9},{9,17},{17,25},{25,1},{2,10},{10... | collective-permute-start | bytes 2359304 | tf_op jit(solution)/shard_map/ppermute | solution.py:13
  1360.3 123.8 %copy-start.3 = (f32[1024]{0:T(1024)S(1)}, f32[1024]{0:T(1024)}, u32[]{:S(2)}) copy-start(f32[1024]{0:T(1024)} %param.19) | copy-start | bytes 12292
  1360.3 123.8 %copy-start.4 = (f32[1024]{0:T(1024)S(1)}, f32[1024]{0:T(1024)}, u32[]{:S(2)}) copy-start(f32[1024]{0:T(1024)} %param.18) | copy-start | bytes 12292
Sparse Core Ops, SparseCore 0:
  9.2 299.7 all-gather.4
  310.9 297.0 all-gather.6
  629.8 110.7 reduce-scatter.2
  742.3 297.5 all-gather.8
  1041.7 297.0 all-gather.10
  1360.5 110.7 reduce-scatter.4
